TPU v7x, 512 devices: a whole 4x8x8 slice. The times are simulated.
512 devices in a mesh: sp: 32 (over z, x), tp: 16 (over y, core).
Axes of the slice: x: 4, y: 8, z: 8, core: 2. Of those that a mesh axis runs over, the one named last changes fastest.
Arguments:
- tokens: bfloat16 [16384, 4096], P('sp', 'tp'), may hold values from -8 to 8
- w_key: bfloat16 [4096, 2048], P(None, 'tp'), may hold values from -0.09375 to 0.09375
- w_value: bfloat16 [4096, 2048], P(None, 'tp'), may hold values from -0.09375 to 0.09375
- w_beta: bfloat16 [4096, 16], replicated, may hold values from -0.09375 to 0.09375
- w_decay: bfloat16 [4096, 16], replicated, may hold values from -0.09375 to 0.09375
- beta_bias: float32 [16], replicated, may hold values from -6 to -4
- decay_rate: float32 [16], replicated, as said below
- forgetting_increment: float32 [16, 16384], P('tp', 'sp')
- new_query: bfloat16 [16, 128], P('tp', 'sp'), may hold values from -6 to 6
- read_gain: bfloat16 [128], replicated, may hold values from 0.099609375 to 1.8984375
Outputs:
- state_cache: bfloat16 [16, 128, 128], P('tp', 'sp')
- first_read: float32 [16, 128], P('tp')
Inputs may be any that keep to these rules, and one draw needn't show every extreme that they name: `decay_rate`: positive.
All inputs are finite; a program needn't handle non-finite values.
Results may differ from a plain program's by a relative error of at most 0.0075.
Values may be sent and summed in bfloat16 or wider, within the bound.
A program may use at most 64 MiB of HBM per device.

v0:
```python
import jax
import jax.numpy as jnp
from jax import lax
from jax.sharding import Mesh
from jax.sharding import PartitionSpec as P

DK = 128
DV = 128
BLOCK = 64
SP = ("sp_0", "sp_1")


norm_eps = 1e-06


def neutral_like(x, identity):
    return jnp.zeros_like(x) + jnp.asarray(identity, x.dtype)


def entering(x, axes, combine, identity):
    before = start = neutral_like(x, identity)
    running = x
    for axis in reversed(axes):
        count, mine = (lax.axis_size(axis), lax.axis_index(axis))
        pieces = lax.all_gather(running, axis)
        inside, running = (start, start)
        for k in reversed(range(count)):
            passed = k > mine
            running = combine(running, pieces[k])
            inside = jnp.where(passed, running, inside)
        before = combine(inside, before)
    return before


def cut_along(x, dim, count):
    lengths = x.shape
    pieces = x.reshape(*lengths[:dim], count, lengths[dim] // count, *lengths[dim + 1 :])
    return jnp.moveaxis(pieces, dim, 0)


def summed_on_arrival(x, axis, dim):
    pieces = cut_along(x, dim, lax.axis_size(axis))
    arrived = lax.all_to_all(pieces, axis, split_axis=0, concat_axis=0, tiled=True)
    return arrived.sum(axis=0)


def from_everyone(x, axis):
    count = lax.axis_size(axis)
    return lax.all_to_all(jnp.broadcast_to(x[None], (count, *x.shape)), axis, 0, 0, tiled=True)


def taken_together(x, axis):
    return from_everyone(x, axis).sum(axis=0)


def matmul_f32(left, right):
    return jnp.dot(left, right, precision=lax.Precision.HIGHEST)


def batched_f32(left, right):
    return jnp.einsum("hij,hjk->hik", left, right, precision=lax.Precision.HIGHEST)


def unit_inverse(lower):
    current_size = lower.shape[0]
    identity = jnp.eye(current_size, dtype=jnp.float32)
    result = identity - lower
    lower_power = lower
    covered = 2
    while covered < current_size:
        lower_power = matmul_f32(lower_power, lower_power)
        result = matmul_f32(result, identity + lower_power)
        covered = covered * 2
    return result


def block_terms(key_blk, value_blk, beta_blk, logd_blk):
    current_size = key_blk.shape[0]
    cumulative = jnp.cumsum(logd_blk)
    spread = cumulative[:, None] - cumulative[None, :]
    location_positions = jnp.arange(current_size)
    causal = location_positions[:, None] >= location_positions[None, :]
    strict = location_positions[:, None] > location_positions[None, :]
    decay_table = jnp.where(causal, jnp.exp(jnp.where(causal, spread, 0.0)), 0.0)
    key_beta = key_blk * beta_blk[:, None]
    lower = jnp.where(strict, matmul_f32(key_beta, key_blk.T) * decay_table, 0.0)
    inverse = unit_inverse(lower)
    update = matmul_f32(inverse, value_blk * beta_blk[:, None])
    erase = matmul_f32(inverse, key_beta * jnp.exp(cumulative)[:, None])
    key_remainder = key_blk * jnp.exp(cumulative[-1] - cumulative)[:, None]
    return (update, erase, key_remainder, jnp.exp(cumulative[-1]))


def per_device(
    tokens,
    w_key,
    w_value,
    w_beta,
    w_decay,
    beta_bias,
    decay_rate,
    forgetting_increment,
    new_query,
    read_gain,
):
    heads_here = w_key.shape[1] // DK
    token_count = tokens.shape[0]
    head_start = lax.axis_index("tp") * heads_here
    gate_weights = jnp.concatenate(
        [
            lax.dynamic_slice_in_dim(w_beta, head_start, heads_here, 1),
            lax.dynamic_slice_in_dim(w_decay, head_start, heads_here, 1),
        ],
        axis=1,
    )
    piece = lax.all_gather(tokens, "tp", axis=1, tiled=True)
    key_acc = jnp.dot(piece, w_key, preferred_element_type=jnp.float32)
    value_acc = jnp.dot(piece, w_value, preferred_element_type=jnp.float32)
    gate_acc = jnp.dot(piece, gate_weights, preferred_element_type=jnp.float32)
    key_wide = (
        lax.optimization_barrier(key_acc.astype(jnp.bfloat16))
        .astype(jnp.float32)
        .reshape(token_count, heads_here, DK)
    )
    key_unit = key_wide * lax.rsqrt(jnp.sum(key_wide * key_wide, axis=-1, keepdims=True) + norm_eps)
    value_wide = (
        lax.optimization_barrier(value_acc.astype(jnp.bfloat16))
        .astype(jnp.float32)
        .reshape(token_count, heads_here, DV)
    )
    bias_here = lax.dynamic_slice_in_dim(beta_bias, head_start, heads_here, 0)
    rate_here = lax.dynamic_slice_in_dim(decay_rate, head_start, heads_here, 0)
    beta = jax.nn.sigmoid(gate_acc[:, :heads_here] + bias_here).T
    log_decay = (
        -rate_here[:, None] * jax.nn.softplus(gate_acc[:, heads_here:].T) + forgetting_increment
    )
    blocks = token_count // BLOCK
    key_heads = key_unit.transpose(1, 0, 2).reshape(heads_here, blocks, BLOCK, DK)
    value_heads = value_wide.transpose(1, 0, 2).reshape(heads_here, blocks, BLOCK, DV)
    terms = jax.vmap(jax.vmap(block_terms))(
        key_heads,
        value_heads,
        beta.reshape(heads_here, blocks, BLOCK),
        log_decay.reshape(heads_here, blocks, BLOCK),
    )
    inputs = tuple((jnp.moveaxis(item, 1, 0) for item in terms))
    identity = jnp.broadcast_to(jnp.eye(DK, dtype=jnp.float32), (heads_here, DK, DK))
    value_zeros = jnp.zeros((heads_here, DK, DV), jnp.float32)
    padding = jnp.zeros((heads_here, BLOCK, DK), jnp.float32)

    def advance(state, block_in):
        update, erase, key_remainder, keep = block_in
        fresh = jnp.concatenate([update, padding], axis=-1) - jnp.einsum(
            "hcd,hde->hce", erase, state, precision=lax.Precision.HIGHEST
        )
        state = keep[:, None, None] * state + jnp.einsum(
            "hcd,hce->hde", key_remainder, fresh, precision=lax.Precision.HIGHEST
        )
        return (state, None)

    combined, _ = lax.scan(advance, jnp.concatenate([value_zeros, identity], axis=-1), inputs)
    local_b = combined[:, :, :DV]
    local_left = combined[:, :, DV:]
    later_product = entering(local_left, SP, batched_f32, identity)
    summed = summed_on_arrival(batched_f32(later_product, local_b), SP, 1)
    own_rows = summed.astype(jnp.bfloat16)
    partial_read = jnp.sum(
        new_query.astype(jnp.float32)[:, :, None] * own_rows.astype(jnp.float32), axis=1
    )
    raw_read = taken_together(partial_read, SP)
    first_read = (
        raw_read
        * lax.rsqrt(jnp.mean(raw_read * raw_read, axis=-1, keepdims=True) + norm_eps)
        * read_gain.astype(jnp.float32)
    )
    return (own_rows, first_read)


def solution(mesh):
    finer = Mesh(mesh.devices.reshape(8, 4, mesh.shape["tp"]), ("sp_0", "sp_1", "tp"))
    return jax.shard_map(
        per_device,
        mesh=finer,
        in_specs=(
            P(SP, "tp"),
            P(None, "tp"),
            P(None, "tp"),
            P(),
            P(),
            P(),
            P(),
            P("tp", SP),
            P("tp", SP),
            P(),
        ),
        out_specs=(P("tp", SP, None), P("tp", None)),
        check_vma=False,
    )
```

profile of v0, /device:TPU:2, one launch (start us, length us, event | category | flops | bytes accessed | tf_op | source)
XLA Modules:
  0.0 179.4 jit_solution(8949332273028373998)
XLA Ops:
  7.2 0.7 all-gather.4.cloned.1.call-update
  8.0 1.2 dynamic_slice.26
  9.8 1.3 dynamic_slice.29
  11.2 0.9 constant_dynamic-slice_fusion.1
  12.1 54.2 %all-gather.4.cloned.1.call-done = bf16[512,4096]{1,0:T(8,128)(2,1)} async-done(((bf16[512,256]{1,0:T(8,128)(2,1)}), bf16[512,4096]{1,0:T(8,128)(2,1)}) %all-gather.4.cloned.1.call-update) | async-done | bytes 4194320 | tf_op jit(solution)/shard_map/all_gather | solution.py:116
  66.3 3.5 %convolution_bitcast_fusion.5 = f32[512,2]{0,1:T(2,128)S(1)} fusion(bf16[512,4096]{1,0:T(8,128)(2,1)} %all-gather.4.cloned.1.call-done, bf16[4096,1]{0,1:T(2,128)(2,1)S(1)} %get-tuple-element.81, bf16[4096,1]{0,1:T(2,128)(2,1)S(1)} %get-tuple-element.82), kind=kOutput, calls=%fused_computation.23 | convolution fusion | flops 8421376 | bytes 4214784 | tf_op jit(solution)/shard_map/dot_general | solution.py:119
  69.7 0.7 fusion.77
  71.1 3.6 %convolution_convert_fusion.1 = bf16[512,128]{1,0:T(8,128)(2,1)S(1)} fusion(bf16[512,4096]{1,0:T(8,128)(2,1)} %all-gather.4.cloned.1.call-done, bf16[4096,128]{1,0:T(8,128)(2,1)S(1)} %copy-done), kind=kOutput, calls=%fused_computation.20 | convolution fusion | flops 536936448 | bytes 5373952 | tf_op jit(solution)/shard_map/dot_general | solution.py:117
  74.7 1.3 convolution_convert_fusion
  76.3 0.6 fusion.10
  82.0 14.6 %while.10 = (s32[]{:T(128)}, f32[1,128,256]{2,1,0:T(8,128)S(1)}, f32[8,1]{0,1:T(1,128)S(1)}, f32[8,1,64,128]{3,2,1,0:T(8,128)S(1)}, f32[8,1,64,128]{3,2,1,0:T(8,...) while((s32[]{:T(128)}, f32[1,128,256]{2,1,0:T(8,128)S(1)}, f32[8,1]{0,1:T(1,128)S(1)}, ...), condition=%wide.region_3.4_spmd, body=%wide.region_2.3_spmd.sunk | while | flops 50413568 | bytes 688241 | solution.py:161
  82.0 0.6 constant_dynamic-slice_fusion.4
  82.9 1.0 fusion.133
  83.9 0.6 constant_dynamic-slice_fusion.4
  84.7 1.0 fusion.133
  85.7 0.6 constant_dynamic-slice_fusion.4
  86.5 1.0 fusion.133
  87.5 0.6 constant_dynamic-slice_fusion.4
  88.3 1.0 fusion.133
  89.4 0.6 constant_dynamic-slice_fusion.4
  90.2 1.0 fusion.133
  91.2 0.6 constant_dynamic-slice_fusion.4
  92.0 1.0 fusion.133
  93.8 1.0 fusion.133
  95.7 1.0 fusion.133
  96.7 12.3 %all-gather = f32[4,128,128]{2,1,0:T(8,128)S(1)} all-gather(f32[1,128,128]{2,1,0:T(8,128)S(1)} %slice.55), channel_id=2, replica_groups=mesh['sp_0'=8,'sp_1'=4,'tp'=16] {'sp_1'}, dimensions={0}, use_global_device_ids=true | all-gather | bytes 327680 | tf_op jit(solution)/shard_map/all_gather | solution.py:25
  109.8 27.8 %all-gather.1 = f32[1024,128]{1,0:T(8,128)S(1)} all-gather(f32[128,128]{1,0:T(8,128)S(1)} %fusion.56), channel_id=3, replica_groups=mesh['sp_0'=8,'sp_1'=4,'tp'=16] {'sp_0'}, dimensions={0}, use_global_device_ids=true | all-gather | bytes 589824 | tf_op jit(solution)/shard_map/all_gather | solution.py:25
  139.9 0.7 copy.34
  140.6 8.3 %all-to-all-start = ((f32[32,1,4,128]{3,2,1,0:T(4,128)}), f32[32,1,4,128]{3,2,1,0:T(4,128)S(1)}, u32[]{:S(2)}, u32[]{:S(2)}) async-start(f32[32,1,4,128]{3,2,1,0:T(4,128)} %copy.34), calls=%async_computation | async-start | bytes 131072 | tf_op jit(solution)/shard_map/all_to_all | solution.py:43
  148.9 8.7 %all-to-all-done = f32[32,1,4,128]{3,2,1,0:T(4,128)S(1)} async-done(((f32[32,1,4,128]{3,2,1,0:T(4,128)}), f32[32,1,4,128]{3,2,1,0:T(4,128)S(1)}, u32[]{:S(2)}, u32[]{:S(2)}) %all-to-all-start) | async-done | bytes 65568 | tf_op jit(solution)/shard_map/all_to_all | solution.py:43
  157.7 12.9 %all_to_all.10 = f32[32,1,128]{2,1,0:T(1,128)S(1)} all-to-all(f32[32,1,128]{2,1,0:T(1,128)S(1)} %broadcast_in_dim.21), channel_id=1, replica_groups=mesh['sp_0'=8,'sp_1'=4,'tp'=16] {'sp_0','sp_1'}, dimensions={0} | all-to-all | bytes 32768 | tf_op jit(solution)/shard_map/all_to_all | solution.py:49
  170.7 0.6 multiply_reduce_fusion.1
  (81 shorter events, 12.6 us)
Async XLA Ops:
  7.2 63.9 %copy-start = (bf16[4096,128]{1,0:T(8,128)(2,1)S(1)}, bf16[4096,128]{1,0:T(8,128)(2,1)}, u32[]{:S(2)}) copy-start(bf16[4096,128]{1,0:T(8,128)(2,1)} %param.13) | copy-start | bytes 3145732
  7.2 63.3 %copy-start.3 = (f32[1,512]{1,0:T(1,128)S(1)}, f32[1,512]{1,0:T(1,128)}, u32[]{:S(2)}) copy-start(f32[1,512]{1,0:T(1,128)} %param.19) | copy-start | bytes 6148
  7.2 59.1 %all-gather.4.cloned.1.call-start = ((), (), s32[]{:S(2)}) async-start(), calls=%async_computation.2 | async-start | bytes 4456448 | tf_op jit(solution)/shard_map/all_gather | solution.py:116
  66.3 8.4 %copy-start.5 = (bf16[4096,128]{1,0:T(8,128)(2,1)S(1)}, bf16[4096,128]{1,0:T(8,128)(2,1)}, u32[]{:S(2)}) copy-start(bf16[4096,128]{1,0:T(8,128)(2,1)} %param.14) | copy-start | bytes 3145732
  70.8 3.9 %copy-start.1 = (bf16[512,4096]{1,0:T(8,128)(2,1)S(1)}, bf16[512,4096]{1,0:T(8,128)(2,1)}, u32[]{:S(2)}) copy-start(bf16[512,4096]{1,0:T(8,128)(2,1)} %all-gather.4.cloned.1.call-done) | copy-start | bytes 12582916
  82.0 66.9 %copy-start.6 = (bf16[1,4]{1,0:T(2,128)(2,1)S(1)}, bf16[1,4]{1,0:T(2,128)(2,1)}, u32[]{:S(2)}) copy-start(bf16[1,4]{1,0:T(2,128)(2,1)} %param.20) | copy-start | bytes 28
  82.0 90.0 %copy-start.4 = (bf16[128]{0:T(256)(128)(2,1)S(1)}, bf16[128]{0:T(256)(128)(2,1)}, u32[]{:S(2)}) copy-start(bf16[128]{0:T(256)(128)(2,1)} %param.21) | copy-start | bytes 772
  140.6 17.0 %all-to-all-start = ((f32[32,1,4,128]{3,2,1,0:T(4,128)}), f32[32,1,4,128]{3,2,1,0:T(4,128)S(1)}, u32[]{:S(2)}, u32[]{:S(2)}) async-start(f32[32,1,4,128]{3,2,1,0:T(4,128)} %copy.34), calls=%async_computation | async-start | bytes 131072 | tf_op jit(solution)/shard_map/all_to_all | solution.py:43
  157.6 14.9 %copy-start.2 = (bf16[4,128]{1,0:T(4,128)(2,1)}, bf16[4,128]{1,0:T(4,128)(2,1)S(1)}, u32[]{:S(2)}) copy-start(bf16[4,128]{1,0:T(4,128)(2,1)S(1)} %reduce_sum.46) | copy-start | bytes 3076
Sparse Core Ops, SparseCore 0:
  10.0 56.1 all-gather.3
where the time goes:
time: 180 us; the launch traced here: 179 us
  waiting for transfers between devices  63.6 us (35%)
  blocking collectives  53 us (29%)
  matrix products  26.5 us (15%)
  between operations  15.8 us (9%)
  local copies, waits for them, and re-layouts  9.17 us (5%)
  starting transfers between devices  8.35 us (5%)
  other arithmetic  2.73 us (2%)
    all_gather x1, waiting for transfers between devices, per_device(): piece = lax.all_gather(tokens, 'tp', axis=1, tiled=True)  54.2 us
    all_gather x2, blocking collectives, entering(): pieces = lax.all_gather(running, axis)  40.1 us
    all_to_all x1, blocking collectives, from_everyone(): lax.all_to_all(jnp.broadcast_to(x[None], (count, *x.shape)), axis, 0, 0,...  12.9 us
    all_to_all x1, waiting for transfers between devices, summed_on_arrival(): lax.all_to_all(pieces, axis, split_axis=0, concat_axis=0, tiled=True)  8.68 us
    all_to_all x1, starting transfers between devices, summed_on_arrival(): lax.all_to_all(pieces, axis, split_axis=0, concat_axis=0, tiled=True)  8.32 us
    dot_general x8, matrix products, advance(): jnp.einsum('hcd,hce->hde', key_remainder, fresh, precision=lax.Precision....  8.06 us
    dot_general x13, matrix products, matmul_f32(): return jnp.dot(left, right, precision=lax.Precision.HIGHEST)  5.49 us
    dynamic_slice x8, local copies, waits for them, and re-layouts, per_device(): lax.scan(advance, jnp.concatenate([value_zeros, identity], axis=-1), inputs)  4.68 us
  transfers between devices with their start and end apart: 2, of which 2 were waited for; matrix products, arithmetic and copies ran while one was open for 2% of the time, Pallas kernels for 0%

commit v1 on v0

v1 whole, which is shorter than its diff:
```python
import functools

import jax
import jax.numpy as jnp
from jax import lax
from jax.experimental import pallas as pl
from jax.experimental.pallas import tpu as pltpu
from jax.sharding import PartitionSpec as P

NX, NZ, NY = 4, 8, 8
G = 4
R = 128
MESH = pl.DeviceIdType.MESH
f32, bf16 = jnp.float32, jnp.bfloat16
norm_eps = 1e-06


def nn(a, b):
    return lax.dot_general(a, b, (((1,), (0,)), ((), ())), preferred_element_type=f32)


def nt(a, b):
    return lax.dot_general(a, b, (((1,), (1,)), ((), ())), preferred_element_type=f32)


def tn(a, b):
    return lax.dot_general(a, b, (((0,), (0,)), ((), ())), preferred_element_type=f32)


def lo(x):
    return x.astype(bf16)


def iota(shape, dim):
    return lax.broadcasted_iota(jnp.int32, shape, dim)


def compose(first, second):
    nb1, a1, nb1_lo = first
    nb2, a2, nb2_lo = second
    q = nn(nb1_lo, nb2_lo[:R])
    n = a2 * nb1[:R] + a1 * nb2[:R] - q[:R]
    b = a2 * nb1[R:] - q[R:] + nb2[R:]
    return n, b, a1 * a2


def joined(n, b, a):
    nb = jnp.concatenate([n, b], axis=0)
    return nb, a, lo(nb)


def block_maps(kvs, gates, fincs, bias, rate):
    count = len(kvs)
    row, col = iota((R, R), 0), iota((R, R), 1)
    strict, causal = row > col, row >= col
    eye = (row == col).astype(f32)
    kw = [kv[:, :R].astype(bf16) for kv in kvs]
    vw = [kv[:, R:].astype(bf16) for kv in kvs]
    kk = [nt(k, k) for k in kw]
    rs = []
    for k in kw:
        wide = k.astype(f32)
        inv = lax.rsqrt(jnp.sum(wide * wide, axis=1, keepdims=True) + norm_eps)
        rs.append(jnp.broadcast_to(inv, (R, R)))
    rs_t = [r.T for r in rs]
    yield None
    beta, cum = [], []
    lane = iota((8, R), 1)
    for (bl, dl), finc in zip(gates, fincs):
        bl = jnp.broadcast_to(bl, (8, R))
        dl = jnp.broadcast_to(dl, (8, R))
        beta.append(jax.nn.sigmoid(bl + bias))
        c = -rate * jax.nn.softplus(dl) + jnp.broadcast_to(finc, (8, R))
        step = 1
        while step < R:
            c = c + jnp.where(lane >= step, pltpu.roll(c, step, 1), 0.0)
            step *= 2
        cum.append(c)
    beta_r = [jnp.broadcast_to(b[:1], (R, R)) for b in beta]
    cum_r = [jnp.broadcast_to(c[:1], (R, R)) for c in cum]
    beta_c = [b.T for b in beta_r]
    cum_c = [c.T for c in cum_r]
    yield None
    lower = []
    for i in range(count):
        spread = jnp.exp(jnp.where(causal, cum_c[i] - cum_r[i], 0.0))
        lower.append(jnp.where(strict, kk[i] * rs[i] * rs_t[i] * beta_c[i] * spread, 0.0))
    same = (row // 16) == (col // 16)
    power = [lo(jnp.where(same, l, 0.0)) for l in lower]
    inverse = [eye - jnp.where(same, l, 0.0) for l in lower]
    for _ in range(3):
        power = [lo(nn(p, p)) for p in power]
        inverse = [x + nn(lo(x), p) for x, p in zip(inverse, power)]
        yield None
    size = 16
    while size < R:
        below = ((row // (2 * size)) == (col // (2 * size))) & ((row // size) > (col // size))
        short = [lo(x) for x in inverse]
        inner = [lo(nn(s, lo(jnp.where(below, l, 0.0)))) for s, l in zip(short, lower)]
        inverse = [x - nn(y, s) for x, y, s in zip(inverse, inner, short)]
        size *= 2
        yield None
    maps = []
    for i in range(count):
        scale_u = beta_r[i]
        scale_e = scale_u * jnp.exp(cum_r[i]) * rs_t[i]
        erase = nn(lo(inverse[i] * scale_e), kw[i])
        update = nn(lo(inverse[i] * scale_u), vw[i])
        last = cum_c[i][R - 1 : R, :]
        remainder = lo(kw[i].astype(f32) * rs[i] * jnp.exp(last - cum_c[i]))
        n = tn(lo(erase), remainder)
        b = tn(lo(update), remainder)
        maps.append(joined(n, b, jnp.exp(last)))
    yield maps


def kernel(
    tok, wk, wv, wb, wd, bias_ref, rate_ref, finc, query, gain,
    state_out, read_out,
    x, wkv, wg, acc, accg, bfull, xs, ps, zs, fs, srow,
    load_sem, rsend, rrecv, dsend, drecv, xsend, xrecv, psem, zsend, zrecv, fsend, frecv,
):
    sp = lax.axis_index("sp")
    tp = lax.axis_index("tp")
    mz, mx = sp // NX, sp % NX
    my, core = tp // 2, tp % 2
    sigma = 2 * (mz % 2) - 1

    def at_y(step):
        return {"sp": sp, "tp": ((my + step + NY) % NY) * 2 + core}

    def at_x(step):
        return {"sp": mz * NX + (mx + step) % NX, "tp": tp}

    def at_z(step):
        return {"sp": ((mz + step + NZ) % NZ) * NX + mx, "tp": tp}

    other_core = {"sp": sp, "tp": my * 2 + 1 - core}
    pair = at_z(1 - 2 * (mz % 2))

    loads = []
    for g in range(G):
        c = pltpu.make_async_copy(
            tok.at[pl.ds(g * R, R)], x.at[tp, pl.ds(g * R, R)], load_sem.at[g]
        )
        c.start()
        loads.append(c)
    weights = [
        pltpu.make_async_copy(wk, wkv.at[:, pl.ds(0, R)], load_sem.at[G]),
        pltpu.make_async_copy(wv, wkv.at[:, pl.ds(R, R)], load_sem.at[G + 1]),
        pltpu.make_async_copy(wb, wg.at[pl.ds(0, 16)], load_sem.at[G + 2]),
        pltpu.make_async_copy(wd, wg.at[pl.ds(16, 16)], load_sem.at[G + 3]),
    ]
    for w in weights:
        w.start()

    barrier = pltpu.get_barrier_semaphore()
    peers = [at_y(1), at_y(-1), other_core, at_x(1), at_x(2), at_x(3)]
    z_peers = [at_z(sigma), at_z(3 * sigma), at_z(2 * sigma), at_z(-2 * sigma)]
    if True:
        z_peers.append(pair)
    for peer in peers + z_peers:
        pl.semaphore_signal(barrier, inc=1, device_id=peer, device_id_type=MESH)
    pl.semaphore_wait(barrier, len(peers) + len(z_peers))

    sent = []

    def shard(way, d, who):
        step = -d if way == 0 else d
        return ((my + step + NY) % NY) * 2 + who

    def rows(g):
        return pl.ds(g * R, R)

    def ring(way, d, g):
        s = shard(way, d, core)
        return pltpu.make_async_remote_copy(
            x.at[s, rows(g)], x.at[s, rows(g)],
            rsend.at[way, d, g], rrecv.at[way, d, g],
            device_id=at_y(1 if way == 0 else -1), device_id_type=MESH,
        )

    def send(way, d, g):
        c = ring(way, d, g)
        c.start()
        sent.append(c)

    def landed(way, d, g):
        s = shard(way, d, core)
        pltpu.make_async_remote_copy(
            x.at[s, rows(g)], x.at[s, rows(g)],
            rsend.at[way, d - 1, g], rrecv.at[way, d - 1, g],
            device_id=at_y(1 if way == 0 else -1), device_id_type=MESH,
        ).wait_recv()

    def across(way, d, g):
        s = shard(way, d, core)
        c = pltpu.make_async_remote_copy(
            x.at[s, rows(g)], x.at[s, rows(g)],
            dsend.at[way, d, g], drecv.at[way, d, g],
            device_id=other_core, device_id_type=MESH,
        )
        c.start()
        sent.append(c)

    def crossed(way, d, g):
        s = shard(way, d, 1 - core)
        pltpu.make_async_remote_copy(
            x.at[s, rows(g)], x.at[s, rows(g)],
            dsend.at[way, d, g], drecv.at[way, d, g],
            device_id=other_core, device_id_type=MESH,
        ).wait_recv()

    def project(items, g, first=False):
        total, gate = None, None
        for s in items:
            piece = x[s, g * R : (g + 1) * R, :]
            at = pl.multiple_of(s * 256, 256)
            p = nn(piece, wkv[pl.ds(at, 256), :])
            q = nt(wg[:, pl.ds(at, 256)], piece)
            total = p if total is None else total + p
            gate = q if gate is None else gate + q
        if first:
            acc[g * R : (g + 1) * R, :] = total
            accg[g] = gate
        else:
            acc[g * R : (g + 1) * R, :] += total
            accg[g] += gate

    pending = []

    def take_pending():
        while pending:
            items, g = pending.pop(0)
            for way, d in items:
                crossed(way, d, g)
            project([shard(way, d, 1 - core) for way, d in items], g)

    def event(items, g, forwards=True):
        for way, d in items:
            landed(way, d, g)
            if forwards and (d < 3 or (d == 3 and g % 2 == way)):
                send(way, d, g)
            across(way, d, g)

    def own_dots(items, g):
        project([shard(way, d, core) for way, d in items], g)
        take_pending()
        pending.append((items, g))

    both = lambda d: [(0, d), (1, d)]

    for g in (0, 1, 2, 3):
        loads[g].wait()
        if g < 3:
            send(0, 0, g)
            send(1, 0, g)
        across(0, 0, g)
    for w in weights:
        w.wait()
    for g in range(G):
        project([tp], g, first=True)

    h = tp
    bias, rate = bias_ref[h], rate_ref[h]

    def blocks_of(groups):
        kvs = [acc[g * R : (g + 1) * R, :] for g in groups]
        gates = [(accg[g, pl.ds(h, 1), :], accg[g, pl.ds(16 + h, 1), :]) for g in groups]
        fincs = [finc[:, g * R : (g + 1) * R] for g in groups]
        return block_maps(kvs, gates, fincs, bias, rate)

    pieces = None
    early = None

    def advance_early(n=1):
        nonlocal early
        for _ in range(n):
            if early is None:
                got = next(pieces)
                if got is not None:
                    early = joined(*compose(got[0], got[1]))

    event(both(1), 0)
    own_dots(both(1), 0)
    pending.append(([(0, 0)], 0))
    event(both(1), 1)
    send(0, 0, 3)
    send(1, 0, 3)
    own_dots(both(1), 1)
    pending.append(([(0, 0)], 1))
    event(both(2), 0)
    own_dots(both(2), 0)
    event(both(2), 1)
    own_dots(both(2), 1)
    event(both(1), 2)
    own_dots(both(1), 2)
    pending.append(([(0, 0)], 2))
    event(both(3), 0)
    event(both(3), 1)
    own_dots(both(3), 0)
    own_dots(both(3), 1)
    event(both(1), 3)
    own_dots(both(1), 3)
    pending.append(([(0, 0)], 3))
    event(both(2), 2)
    own_dots(both(2), 2)
    take_pending()
    event([(0, 4)], 0)
    event([(1, 4)], 1)
    own_dots([(0, 4)], 0)
    own_dots([(1, 4)], 1)
    take_pending()
    pieces = blocks_of((0, 1))
    advance_early(2)
    event(both(2), 3)
    own_dots(both(2), 3)
    advance_early(3)
    event(both(3), 2)
    own_dots(both(3), 2)
    advance_early(4)
    event(both(3), 3)
    own_dots(both(3), 3)
    take_pending()
    advance_early(4)
    event([(0, 4)], 2)
    event([(1, 4)], 3)
    own_dots([(0, 4)], 2)
    own_dots([(1, 4)], 3)
    take_pending()
    late = None
    for got in blocks_of((2, 3)):
        late = got
    n, b, a = compose(early, joined(*compose(late[0], late[1])))

    def keep_rows(keep, qrow):
        hi = keep.astype(bf16).astype(f32)
        mid = (keep - hi).astype(bf16).astype(f32)
        rest = keep - hi - mid
        r16 = iota((16, R), 0)
        blk = jnp.where(r16 == 0, hi, jnp.where(r16 == 1, mid, jnp.where(r16 == 2, rest, 0.0)))
        return lo(jnp.where(r16 == 3, qrow, blk))

    lane1 = iota((1, R), 1)
    q4 = query[...].astype(f32)
    qrow = jnp.zeros((1, R), f32)
    for i in range(4):
        qrow = qrow + jnp.where(lane1 == 4 * sp + i, q4[:, i : i + 1], 0.0)
    xs[mx, 0:R, :] = lo(n)
    xs[mx, R : R + 16, :] = keep_rows(a, qrow)
    bfull[...] = lo(b).reshape(NX, 32, R)
    sent_x = []
    for o in (2, 1, 3):
        c = pltpu.make_async_remote_copy(
            xs.at[mx, pl.ds(0, R + 16)], xs.at[mx, pl.ds(0, R + 16)],
            xsend.at[0, o - 1], xrecv.at[0, o - 1], device_id=at_x(o), device_id_type=MESH,
        )
        c.start()
        sent_x.append(c)
        c = pltpu.make_async_remote_copy(
            bfull.at[(mx + o) % NX], xs.at[mx, pl.ds(R + 16, 32)],
            xsend.at[1, o - 1], xrecv.at[1, o - 1], device_id=at_x(o), device_id_type=MESH,
        )
        c.start()
        sent_x.append(c)
    xs[mx, R + 16 : R + 48, :] = bfull[mx]

    def unpack(ref, k):
        n_lo = ref[k, 0:R, :]
        extra = ref[k, R : R + 16, :].astype(f32)
        b_lo = ref[k, R + 16 : R + 48, :]
        keep = extra[0:1] + extra[1:2] + extra[2:3]
        nb_lo = jnp.concatenate([n_lo, b_lo], axis=0)
        return (nb_lo.astype(f32), keep, nb_lo), extra[3:4]

    for o in (1, 3, 2):
        src = (mx + NX - o) % NX
        pltpu.make_async_remote_copy(
            xs.at[src, pl.ds(0, R + 16)], xs.at[src, pl.ds(0, R + 16)],
            xsend.at[0, o - 1], xrecv.at[0, o - 1], device_id=at_x(o), device_id_type=MESH,
        ).wait_recv()
        pltpu.make_async_remote_copy(
            bfull.at[0], xs.at[src, pl.ds(R + 16, 32)],
            xsend.at[1, o - 1], xrecv.at[1, o - 1], device_id=at_x(o), device_id_type=MESH,
        ).wait_recv()
    got = [unpack(xs, k) for k in range(NX)]
    half0 = joined(*compose(got[0][0], got[1][0]))
    half1 = joined(*compose(got[2][0], got[3][0]))
    n, b, a = compose(half0, half1)
    qrow = got[0][1] + got[1][1] + got[2][1] + got[3][1]

    def put(ref, slot, n, b, a, qrow):
        ref[slot, 0:R, :] = lo(n)
        ref[slot, R : R + 16, :] = keep_rows(a, qrow)
        ref[slot, R + 16 : R + 48, :] = lo(b)

    me2 = mz % 2
    put(ps, me2, n, b, a, qrow)
    c = pltpu.make_async_remote_copy(
        ps.at[me2], ps.at[me2], psem.at[0], psem.at[1], device_id=pair, device_id_type=MESH
    )
    c.start()
    sent_x.append(c)
    pltpu.make_async_remote_copy(
        ps.at[1 - me2], ps.at[1 - me2], psem.at[0], psem.at[1], device_id=pair, device_id_type=MESH
    ).wait_recv()
    got = [unpack(ps, k) for k in range(2)]
    n, b, a = compose(got[0][0], got[1][0])
    qrow = got[0][1] + got[1][1]

    mine = mz // 2
    put(zs, mine, n, b, a, qrow)
    for o in (3, 2, 1):
        c = pltpu.make_async_remote_copy(
            zs.at[mine], zs.at[mine], zsend.at[o - 1], zrecv.at[o - 1],
            device_id=at_z(o * sigma), device_id_type=MESH,
        )
        c.start()
        sent_x.append(c)
    for o, step in ((1, 1), (2, -2), (3, 3)):
        src = ((mz + step * sigma + NZ) % NZ) // 2
        pltpu.make_async_remote_copy(
            zs.at[src], zs.at[src], zsend.at[o - 1], zrecv.at[o - 1],
            device_id=at_z(o * sigma), device_id_type=MESH,
        ).wait_recv()
    got = [unpack(zs, k) for k in range(4)]
    state = got[0][0][0][R:]
    for k in range(1, 4):
        nb, keep, nb_lo = got[k][0]
        state = keep * state - nn(lo(state), nb_lo[:R]) + nb[R:]
    qrow = got[0][1] + got[1][1] + got[2][1] + got[3][1]

    fs[mx] = lo(state)
    for o in (2, 1, 3):
        c = pltpu.make_async_remote_copy(
            fs.at[mx], fs.at[mx], fsend.at[o - 1], frecv.at[o - 1],
            device_id=at_x(o), device_id_type=MESH,
        )
        c.start()
        sent_x.append(c)
    for o in (1, 3, 2):
        src = (mx + NX - o) % NX
        pltpu.make_async_remote_copy(
            fs.at[src], fs.at[src], fsend.at[o - 1], frecv.at[o - 1],
            device_id=at_x(o), device_id_type=MESH,
        ).wait_recv()
    whole = fs[...].reshape(R, R)
    raw = nt(jnp.broadcast_to(lo(qrow), (16, R)), whole)[0:1]
    gains = gain[...].astype(f32)
    read_out[...] = raw * lax.rsqrt(jnp.mean(raw * raw, axis=1, keepdims=True) + norm_eps) * gains
    srow[...] = whole.astype(f32).T
    state_out[0] = lo(srow[pl.ds(pl.multiple_of(4 * sp, 4), 4), :])

    for c in sent + sent_x:
        c.wait_send()


def per_device(tokens, w_key, w_value, w_beta, w_decay, beta_bias, decay_rate, finc, query, gain):
    hbm = pl.BlockSpec(memory_space=pl.ANY)
    vmem = pl.BlockSpec(memory_space=pltpu.VMEM)
    smem = pl.BlockSpec(memory_space=pltpu.SMEM)
    dma = pltpu.SemaphoreType.DMA
    return pl.pallas_call(
        kernel,
        out_shape=(
            jax.ShapeDtypeStruct((1, 4, R), bf16),
            jax.ShapeDtypeStruct((1, R), f32),
        ),
        in_specs=[hbm] * 5 + [smem, smem, vmem, vmem, vmem],
        out_specs=(vmem, vmem),
        scratch_shapes=[
            pltpu.VMEM((16, G * R, 256), bf16),
            pltpu.VMEM((4096, 256), bf16),
            pltpu.VMEM((32, 4096), bf16),
            pltpu.VMEM((G * R, 256), f32),
            pltpu.VMEM((G, 32, R), f32),
            pltpu.VMEM((NX, 32, R), bf16),
            pltpu.VMEM((NX, 176, R), bf16),
            pltpu.VMEM((2, 176, R), bf16),
            pltpu.VMEM((4, 176, R), bf16),
            pltpu.VMEM((NX, 32, R), bf16),
            pltpu.VMEM((R, R), f32),
            dma((G + 4,)),
            dma((2, 4, G)), dma((2, 4, G)),
            dma((2, 5, G)), dma((2, 5, G)),
            dma((2, 3)), dma((2, 3)),
            dma((2,)),
            dma((3,)), dma((3,)),
            dma((3,)), dma((3,)),
        ],
        compiler_params=pltpu.CompilerParams(
            collective_id=0, has_side_effects=True, vmem_limit_bytes=60 * 2**20
        ),
    )(
        tokens, w_key, w_value, w_beta.T, w_decay.T, beta_bias, decay_rate, finc, query,
        gain.reshape(1, R),
    )


def solution(mesh):
    return jax.shard_map(
        per_device,
        mesh=mesh,
        in_specs=(
            P("sp", "tp"),
            P(None, "tp"),
            P(None, "tp"),
            P(),
            P(),
            P(),
            P(),
            P("tp", "sp"),
            P("tp", "sp"),
            P(),
        ),
        out_specs=(P("tp", "sp", None), P("tp", None)),
        check_vma=False,
    )
```

time: 180 us -> 66.6 us (0.37)
  Pallas kernels: 0 us -> 63.9 us
  waiting for transfers between devices: 63.6 us -> 0 us
  blocking collectives: 53 us -> 0 us
  matrix products: 26.5 us -> 0 us
  between operations: 15.8 us -> 0.65 us
  starting transfers between devices: 8.35 us -> 0 us
  local copies, waits for them, and re-layouts: 9.17 us -> 1.8 us
  other arithmetic: 2.73 us -> 0 us
    pallas_call x0 -> x1, Pallas kernels: none -> 63.9 us  [per_device(): pl.pallas_call(kernel, out_shape=(jax.ShapeDtypeStruct((1, 4, R), bf16),...]
    all_gather x1 -> x0, waiting for transfers between devices: 54.2 us -> none  [per_device(): piece = lax.all_gather(tokens, 'tp', axis=1, tiled=True)]
    all_gather x2 -> x0, blocking collectives: 40.1 us -> none  [entering(): pieces = lax.all_gather(running, axis)]
    dot_general x47 -> x0, matrix products: 26.5 us -> none  [the longest x8 8.06 us: advance(): jnp.einsum('hcd,hce->hde', key_remainder, fresh, precision=lax.Precision....]
    all_to_all x1 -> x0, blocking collectives: 12.9 us -> none  [from_everyone(): lax.all_to_all(jnp.broadcast_to(x[None], (count, *x.shape)), axis, 0, 0,...]
    all_to_all x1 -> x0, waiting for transfers between devices: 8.68 us -> none  [summed_on_arrival(): lax.all_to_all(pieces, axis, split_axis=0, concat_axis=0, tiled=True)]
    all_to_all x1 -> x0, starting transfers between devices: 8.32 us -> none  [summed_on_arrival(): lax.all_to_all(pieces, axis, split_axis=0, concat_axis=0, tiled=True)]
    dynamic_slice x11 -> x0, local copies, waits for them, and re-layouts: 8.09 us -> none  [the longest x8 4.68 us: per_device(): lax.scan(advance, jnp.concatenate([value_zeros, identity], axis=-1), inputs)]
  transfers between devices with their start and end apart: 2 -> 0, of which waited for: 2 -> 0; matrix products, arithmetic and copies ran while one was open for 2% -> 0% of each run, Pallas kernels for 0% -> 0%
where the time goes in v1:
time: 66.6 us; the launch traced here: 66.4 us
  Pallas kernels  63.9 us (96%)
  local copies, waits for them, and re-layouts  1.8 us (3%)
    pallas_call x1, Pallas kernels, per_device(): pl.pallas_call(kernel, out_shape=(jax.ShapeDtypeStruct((1, 4, R), bf16),...  63.9 us
    unnamed x6, local copies, waits for them, and re-layouts  1.8 us

profile of v1, /device:TPU:2, one launch (start us, length us, event | category | flops | bytes accessed | tf_op | source)
XLA Modules:
  0.0 66.4 jit_solution(17000628881111968801)
XLA Ops:
  0.6 63.9 %shard_map.113 = (bf16[1,4,128]{2,1,0:T(4,128)(2,1)}, f32[1,128]{1,0:T(1,128)}) custom-call(bf16[512,256]{1,0:T(8,128)(2,1)} %tok.1, bf16[4096,128]{1,0:T(8,128)(2,1)} %wk.1, bf16[4096,128]{1,0:T(8,128)(2,1)} %wv.1, bf16[16,4096]{1,0:T(8,128)(2,1)} %bitcast.3, bf16[16,4096]{1,0:T(8,128)(2,1)} %bitcast.4, f32[16]{0:T(128)} %bias_ref.1, f32[16]{0:T(128)} %rate_ref.1, ...), custom_call_target="tpu_custom_call" | custom-call | tf_op jit(solution)/shard_map/pallas_call | solution.py:463
  64.6 0.0 copy-start
  64.6 0.7 copy-done
  65.3 0.0 copy-start.1
  65.3 0.6 copy.14
  65.8 0.1 copy-done.1
  65.9 0.5 copy.15
Async XLA Ops:
  64.6 0.7 %copy-start = (bf16[1,4,128]{2,1,0:T(4,128)(2,1)S(1)}, bf16[1,4,128]{2,1,0:T(4,128)(2,1)}, u32[]{:S(2)}) copy-start(bf16[1,4,128]{2,1,0:T(4,128)(2,1)} %get-tuple-element.4) | copy-start | bytes 3076
  65.3 0.6 copy-start.1

commit v2 on v1

--- a/solution.py
+++ b/solution.py
@@ -115,8 +115,9 @@
 
 
 def kernel(
-    tok, wk, wv, wb, wd, bias_ref, rate_ref, finc, query, gain,
-    state_out, read_out,
+    tok, wk, wv, wb, wd, bias_in, rate_in, finc_in, query_in, gain_in,
+    packed,
+    bias_ref, rate_ref, finc, query, gain,
     x, wkv, wg, acc, accg, bfull, xs, ps, zs, fs, srow,
     load_sem, rsend, rrecv, dsend, drecv, xsend, xrecv, psem, zsend, zrecv, fsend, frecv,
 ):
@@ -151,7 +152,14 @@
         pltpu.make_async_copy(wb, wg.at[pl.ds(0, 16)], load_sem.at[G + 2]),
         pltpu.make_async_copy(wd, wg.at[pl.ds(16, 16)], load_sem.at[G + 3]),
     ]
-    for w in weights:
+    smalls = [
+        pltpu.make_async_copy(src, dst, load_sem.at[G + 4 + i])
+        for i, (src, dst) in enumerate((
+            (bias_in, bias_ref), (rate_in, rate_ref), (finc_in, finc),
+            (query_in, query), (gain_in, gain),
+        ))
+    ]
+    for w in weights + smalls:
         w.start()
 
     barrier = pltpu.get_barrier_semaphore()
@@ -172,24 +180,19 @@
     def rows(g):
         return pl.ds(g * R, R)
 
-    def ring(way, d, g):
+    def ring(way, d, g, sub):
         s = shard(way, d, core)
+        part = x.at[s, pl.ds(g * R + sub * (R // 2), R // 2)]
         return pltpu.make_async_remote_copy(
-            x.at[s, rows(g)], x.at[s, rows(g)],
-            rsend.at[way, d, g], rrecv.at[way, d, g],
+            part, part, rsend.at[way, d, 2 * g + sub], rrecv.at[way, d, 2 * g + sub],
             device_id=at_y(1 if way == 0 else -1), device_id_type=MESH,
         )
 
-    def send(way, d, g):
-        c = ring(way, d, g)
-        c.start()
-        sent.append(c)
-
-    def landed(way, d, g):
+    def landed(way, d, g, sub):
         s = shard(way, d, core)
+        part = x.at[s, pl.ds(g * R + sub * (R // 2), R // 2)]
         pltpu.make_async_remote_copy(
-            x.at[s, rows(g)], x.at[s, rows(g)],
-            rsend.at[way, d - 1, g], rrecv.at[way, d - 1, g],
+            part, part, rsend.at[way, d - 1, 2 * g + sub], rrecv.at[way, d - 1, 2 * g + sub],
             device_id=at_y(1 if way == 0 else -1), device_id_type=MESH,
         ).wait_recv()
 
@@ -229,37 +232,55 @@
 
     pending = []
 
-    def take_pending():
-        while pending:
-            items, g = pending.pop(0)
-            for way, d in items:
-                crossed(way, d, g)
-            project([shard(way, d, 1 - core) for way, d in items], g)
-
-    def event(items, g, forwards=True):
-        for way, d in items:
-            landed(way, d, g)
-            if forwards and (d < 3 or (d == 3 and g % 2 == way)):
-                send(way, d, g)
-            across(way, d, g)
-
-    def own_dots(items, g):
-        project([shard(way, d, core) for way, d in items], g)
-        take_pending()
-        pending.append((items, g))
-
-    both = lambda d: [(0, d), (1, d)]
-
-    for g in (0, 1, 2, 3):
-        loads[g].wait()
-        if g < 3:
-            send(0, 0, g)
-            send(1, 0, g)
-        across(0, 0, g)
-    for w in weights:
+    def take_pending(leave=0):
+        while len(pending) > leave:
+            way, d, g = pending.pop(0)
+            crossed(way, d, g)
+            project([shard(way, d, 1 - core)], g)
+
+    def event(way, d, g, forward):
+        for sub in range(2):
+            landed(way, d, g, sub)
+            if forward:
+                c = ring(way, d, g, sub)
+                c.start()
+                sent.append(c)
+        across(way, d, g)
+
+    def step(d, half, leave=4):
+        todo = []
+        for way in range(2):
+            g = half if way == 0 else half ^ 1
+            event(way, d, g, d < 3 or (d == 3 and half % 2 == 0))
+            todo.append((way, d, g))
+        for way, d, g in todo:
+            project([shard(way, d, core)], g)
+            pending.append((way, d, g))
+        take_pending(leave)
+
+    def own(half):
+        for way in range(2):
+            g = half if way == 0 else half ^ 1
+            for sub in range(2):
+                c = ring(way, 0, g, sub)
+                c.start()
+                sent.append(c)
+
+    loads[0].wait()
+    loads[1].wait()
+    own(0)
+    own(1)
+    across(0, 0, 0)
+    across(0, 0, 1)
+    loads[2].wait()
+    loads[3].wait()
+    across(0, 0, 2)
+    across(0, 0, 3)
+    for w in weights + smalls:
         w.wait()
     for g in range(G):
         project([tp], g, first=True)
+        pending.append((0, 0, g))
 
     h = tp
     bias, rate = bias_ref[h], rate_ref[h]
@@ -270,68 +291,28 @@
         fincs = [finc[:, g * R : (g + 1) * R] for g in groups]
         return block_maps(kvs, gates, fincs, bias, rate)
 
-    pieces = None
-    early = None
-
-    def advance_early(n=1):
-        nonlocal early
-        for _ in range(n):
-            if early is None:
-                got = next(pieces)
-                if got is not None:
-                    early = joined(*compose(got[0], got[1]))
-
-    event(both(1), 0)
-    own_dots(both(1), 0)
-    pending.append(([(0, 0)], 0))
-    event(both(1), 1)
-    send(0, 0, 3)
-    send(1, 0, 3)
-    own_dots(both(1), 1)
-    pending.append(([(0, 0)], 1))
-    event(both(2), 0)
-    own_dots(both(2), 0)
-    event(both(2), 1)
-    own_dots(both(2), 1)
-    event(both(1), 2)
-    own_dots(both(1), 2)
-    pending.append(([(0, 0)], 2))
-    event(both(3), 0)
-    event(both(3), 1)
-    own_dots(both(3), 0)
-    own_dots(both(3), 1)
-    event(both(1), 3)
-    own_dots(both(1), 3)
-    pending.append(([(0, 0)], 3))
-    event(both(2), 2)
-    own_dots(both(2), 2)
-    take_pending()
-    event([(0, 4)], 0)
-    event([(1, 4)], 1)
-    own_dots([(0, 4)], 0)
-    own_dots([(1, 4)], 1)
-    take_pending()
-    pieces = blocks_of((0, 1))
-    advance_early(2)
-    event(both(2), 3)
-    own_dots(both(2), 3)
-    advance_early(3)
-    event(both(3), 2)
-    own_dots(both(3), 2)
-    advance_early(4)
-    event(both(3), 3)
-    own_dots(both(3), 3)
-    take_pending()
-    advance_early(4)
-    event([(0, 4)], 2)
-    event([(1, 4)], 3)
-    own_dots([(0, 4)], 2)
-    own_dots([(1, 4)], 3)
+    own(2)
+    own(3)
+    step(1, 0, 6)
+    step(1, 1, 6)
+    step(1, 2, 6)
+    step(1, 3, 6)
+    step(2, 0, 6)
+    step(2, 1, 6)
+    step(2, 2, 6)
+    step(2, 3, 6)
+    step(3, 0, 6)
+    step(3, 1, 6)
+    step(3, 2, 6)
+    step(3, 3, 6)
+    step(4, 0, 4)
+    step(4, 2, 4)
     take_pending()
     late = None
-    for got in blocks_of((2, 3)):
+    for got in blocks_of((0, 1, 2, 3)):
         late = got
-    n, b, a = compose(early, joined(*compose(late[0], late[1])))
+    early = joined(*compose(late[0], late[1]))
+    n, b, a = compose(early, joined(*compose(late[2], late[3])))
 
     def keep_rows(keep, qrow):
         hi = keep.astype(bf16).astype(f32)
@@ -447,28 +428,35 @@
     whole = fs[...].reshape(R, R)
     raw = nt(jnp.broadcast_to(lo(qrow), (16, R)), whole)[0:1]
     gains = gain[...].astype(f32)
-    read_out[...] = raw * lax.rsqrt(jnp.mean(raw * raw, axis=1, keepdims=True) + norm_eps) * gains
+    read = raw * lax.rsqrt(jnp.mean(raw * raw, axis=1, keepdims=True) + norm_eps) * gains
     srow[...] = whole.astype(f32).T
-    state_out[0] = lo(srow[pl.ds(pl.multiple_of(4 * sp, 4), 4), :])
+    packed[0:4, :] = srow[pl.ds(pl.multiple_of(4 * sp, 4), 4), :]
+    packed[4:5, :] = read
 
     for c in sent + sent_x:
         c.wait_send()
+
+
+def unpack_out(packed, state_out, read_out):
+    state_out[0] = lo(packed[0:4, :])
+    read_out[...] = packed[4:5, :]
 
 
 def per_device(tokens, w_key, w_value, w_beta, w_decay, beta_bias, decay_rate, finc, query, gain):
     hbm = pl.BlockSpec(memory_space=pl.ANY)
     vmem = pl.BlockSpec(memory_space=pltpu.VMEM)
-    smem = pl.BlockSpec(memory_space=pltpu.SMEM)
     dma = pltpu.SemaphoreType.DMA
-    return pl.pallas_call(
+    packed = pl.pallas_call(
         kernel,
-        out_shape=(
-            jax.ShapeDtypeStruct((1, 4, R), bf16),
-            jax.ShapeDtypeStruct((1, R), f32),
-        ),
-        in_specs=[hbm] * 5 + [smem, smem, vmem, vmem, vmem],
-        out_specs=(vmem, vmem),
+        out_shape=jax.ShapeDtypeStruct((8, R), f32),
+        in_specs=[hbm] * 10,
+        out_specs=vmem,
         scratch_shapes=[
+            pltpu.SMEM((16,), f32),
+            pltpu.SMEM((16,), f32),
+            pltpu.VMEM((1, G * R), f32),
+            pltpu.VMEM((1, 4), bf16),
+            pltpu.VMEM((1, R), bf16),
             pltpu.VMEM((16, G * R, 256), bf16),
             pltpu.VMEM((4096, 256), bf16),
             pltpu.VMEM((32, 4096), bf16),
@@ -480,8 +468,8 @@
             pltpu.VMEM((4, 176, R), bf16),
             pltpu.VMEM((NX, 32, R), bf16),
             pltpu.VMEM((R, R), f32),
-            dma((G + 4,)),
-            dma((2, 4, G)), dma((2, 4, G)),
+            dma((G + 9,)),
+            dma((2, 4, 2 * G)), dma((2, 4, 2 * G)),
             dma((2, 5, G)), dma((2, 5, G)),
             dma((2, 3)), dma((2, 3)),
             dma((2,)),
@@ -495,6 +483,15 @@
         tokens, w_key, w_value, w_beta.T, w_decay.T, beta_bias, decay_rate, finc, query,
         gain.reshape(1, R),
     )
+    return pl.pallas_call(
+        unpack_out,
+        out_shape=(
+            jax.ShapeDtypeStruct((1, 4, R), bf16),
+            jax.ShapeDtypeStruct((1, R), f32),
+        ),
+        in_specs=[vmem],
+        out_specs=(vmem, vmem),
+    )(packed)
 
 
 def solution(mesh):

time: 66.6 us -> 61.2 us (0.919)
  Pallas kernels: 63.9 us -> 60.4 us
  local copies, waits for them, and re-layouts: 1.8 us -> 0 us
    pallas_call x1 -> x2, Pallas kernels: 63.9 us -> 60.4 us  [the longest x1 59.1 us: per_device(): pl.pallas_call(kernel, out_shape=jax.ShapeDtypeStruct((8, R), f32), in_sp...]
    unnamed x6 -> x0, local copies, waits for them, and re-layouts: 1.8 us -> none
where the time goes in v2:
time: 61.2 us; the launch traced here: 61 us
  Pallas kernels  60.4 us (99%)
  between operations  0.64 us (1%)
    pallas_call x1, Pallas kernels, per_device(): pl.pallas_call(kernel, out_shape=jax.ShapeDtypeStruct((8, R), f32), in_sp...  59.1 us
    pallas_call x1, Pallas kernels, per_device(): pl.pallas_call(unpack_out, out_shape=(jax.ShapeDtypeStruct((1, 4, R), bf1...  1.25 us

profile of v2, /device:TPU:2, one launch (start us, length us, event | category | flops | bytes accessed | tf_op | source)
XLA Modules:
  0.0 61.0 jit_solution(17454863198495061270)
XLA Ops:
  0.6 59.1 %shard_map.113.packed = f32[8,128]{1,0:T(8,128)} custom-call(bf16[512,256]{1,0:T(8,128)(2,1)} %tok.1, bf16[4096,128]{1,0:T(8,128)(2,1)} %wk.1, bf16[4096,128]{1,0:T(8,128)(2,1)} %wv.1, bf16[16,4096]{1,0:T(8,128)(2,1)} %bitcast.3, bf16[16,4096]{1,0:T(8,128)(2,1)} %bitcast.4, f32[16]{0:T(128)} %bias_in.1, f32[16]{0:T(128)} %rate_in.1, f32[1,512]{1,0:T(1,128)} %finc_in.1, ...), custom_call_target="tpu_custom_call" | custom-call | tf_op jit(solution)/shard_map/pallas_call | solution.py:449
  59.8 1.3 %shard_map.114 = (bf16[1,4,128]{2,1,0:T(4,128)(2,1)}, f32[1,128]{1,0:T(1,128)}) custom-call(f32[8,128]{1,0:T(8,128)} %shard_map.113.packed), custom_call_target="tpu_custom_call" | custom-call | tf_op jit(solution)/shard_map/pallas_call | solution.py:486

commit v3 on v2

--- a/solution.py
+++ b/solution.py
@@ -52,46 +52,41 @@
 def block_maps(kvs, gates, fincs, bias, rate):
     count = len(kvs)
     row, col = iota((R, R), 0), iota((R, R), 1)
-    strict, causal = row > col, row >= col
+    strict = row > col
     eye = (row == col).astype(f32)
     kw = [kv[:, :R].astype(bf16) for kv in kvs]
-    vw = [kv[:, R:].astype(bf16) for kv in kvs]
     kk = [nt(k, k) for k in kw]
-    rs = []
-    for k in kw:
+    logits = jnp.concatenate([dl for _, dl in gates] + [bl for bl, _ in gates], axis=0)
+    c = -rate * jax.nn.softplus(logits) + jnp.concatenate(fincs + fincs, axis=0)
+    beta = jax.nn.sigmoid(logits + bias)
+    lane = iota((2 * count, R), 1)
+    step = 1
+    while step < R:
+        c = c + jnp.where(lane >= step, pltpu.roll(c, step, 1), 0.0)
+        step *= 2
+    packed = jnp.where(iota((2 * count, R), 0) < count, c, beta)
+    columns = packed.T
+    rs, spread_rs = [], jnp.zeros((R, R), f32)
+    for i, k in enumerate(kw):
         wide = k.astype(f32)
-        inv = lax.rsqrt(jnp.sum(wide * wide, axis=1, keepdims=True) + norm_eps)
-        rs.append(jnp.broadcast_to(inv, (R, R)))
-    rs_t = [r.T for r in rs]
-    yield None
-    beta, cum = [], []
-    lane = iota((8, R), 1)
-    for (bl, dl), finc in zip(gates, fincs):
-        bl = jnp.broadcast_to(bl, (8, R))
-        dl = jnp.broadcast_to(dl, (8, R))
-        beta.append(jax.nn.sigmoid(bl + bias))
-        c = -rate * jax.nn.softplus(dl) + jnp.broadcast_to(finc, (8, R))
-        step = 1
-        while step < R:
-            c = c + jnp.where(lane >= step, pltpu.roll(c, step, 1), 0.0)
-            step *= 2
-        cum.append(c)
-    beta_r = [jnp.broadcast_to(b[:1], (R, R)) for b in beta]
-    cum_r = [jnp.broadcast_to(c[:1], (R, R)) for c in cum]
-    beta_c = [b.T for b in beta_r]
-    cum_c = [c.T for c in cum_r]
-    yield None
+        rs.append(lax.rsqrt(jnp.sum(wide * wide, axis=1, keepdims=True) + norm_eps))
+        spread_rs = jnp.where(col == i, rs[i], spread_rs)
+    rs_rows = spread_rs.T
+    cum_r = [packed[i : i + 1] for i in range(count)]
+    cum_c = [columns[:, i : i + 1] for i in range(count)]
+    beta_r = [packed[count + i : count + i + 1] for i in range(count)]
+    beta_c = [columns[:, count + i : count + i + 1] for i in range(count)]
+    rs_r = [rs_rows[i : i + 1] for i in range(count)]
     lower = []
     for i in range(count):
-        spread = jnp.exp(jnp.where(causal, cum_c[i] - cum_r[i], 0.0))
-        lower.append(jnp.where(strict, kk[i] * rs[i] * rs_t[i] * beta_c[i] * spread, 0.0))
+        decay = jnp.exp(jnp.where(strict, cum_c[i] - cum_r[i], 0.0))
+        lower.append(jnp.where(strict, kk[i] * (rs[i] * beta_c[i]) * rs_r[i] * decay, 0.0))
     same = (row // 16) == (col // 16)
     power = [lo(jnp.where(same, l, 0.0)) for l in lower]
     inverse = [eye - jnp.where(same, l, 0.0) for l in lower]
     for _ in range(3):
         power = [lo(nn(p, p)) for p in power]
         inverse = [x + nn(lo(x), p) for x, p in zip(inverse, power)]
-        yield None
     size = 16
     while size < R:
         below = ((row // (2 * size)) == (col // (2 * size))) & ((row // size) > (col // size))
@@ -99,19 +94,22 @@
         inner = [lo(nn(s, lo(jnp.where(below, l, 0.0)))) for s, l in zip(short, lower)]
         inverse = [x - nn(y, s) for x, y, s in zip(inverse, inner, short)]
         size *= 2
-        yield None
-    maps = []
+    ns, keeps, remainders = [], [], []
     for i in range(count):
-        scale_u = beta_r[i]
-        scale_e = scale_u * jnp.exp(cum_r[i]) * rs_t[i]
-        erase = nn(lo(inverse[i] * scale_e), kw[i])
-        update = nn(lo(inverse[i] * scale_u), vw[i])
-        last = cum_c[i][R - 1 : R, :]
-        remainder = lo(kw[i].astype(f32) * rs[i] * jnp.exp(last - cum_c[i]))
-        n = tn(lo(erase), remainder)
-        b = tn(lo(update), remainder)
-        maps.append(joined(n, b, jnp.exp(last)))
-    yield maps
+        last = cum_r[i][:, R - 1 : R]
+        keeps.append(jnp.broadcast_to(jnp.exp(last), (1, R)))
+        remainders.append(lo(kw[i].astype(f32) * (rs[i] * jnp.exp(last - cum_c[i]))))
+        erase = nn(lo(inverse[i] * (beta_r[i] * jnp.exp(cum_r[i]) * rs_r[i])), kw[i])
+        ns.append(tn(lo(erase), remainders[i]))
+
+    def values():
+        bs = []
+        for i in range(count):
+            update = nn(lo(inverse[i] * beta_r[i]), kvs[i][:, R:].astype(bf16))
+            bs.append(tn(lo(update), remainders[i]))
+        return bs
+
+    return ns, keeps, values
 
 
 def kernel(
@@ -159,8 +157,6 @@
             (query_in, query), (gain_in, gain),
         ))
     ]
-    for w in weights + smalls:
-        w.start()
 
     barrier = pltpu.get_barrier_semaphore()
     peers = [at_y(1), at_y(-1), other_core, at_x(1), at_x(2), at_x(3)]
@@ -272,6 +268,8 @@
     own(1)
     across(0, 0, 0)
     across(0, 0, 1)
+    for w in weights + smalls:
+        w.start()
     loads[2].wait()
     loads[3].wait()
     across(0, 0, 2)
@@ -309,10 +307,14 @@
     step(4, 2, 4)
     take_pending()
     late = None
-    for got in blocks_of((0, 1, 2, 3)):
-        late = got
-    early = joined(*compose(late[0], late[1]))
-    n, b, a = compose(early, joined(*compose(late[2], late[3])))
+    ns, keeps, values = blocks_of((0, 1, 2, 3))
+
+    def n_of(n1, a1, n2, a2):
+        return a2 * n1 + a1 * n2 - nn(lo(n1), lo(n2))
+
+    n01, a01 = n_of(ns[0], keeps[0], ns[1], keeps[1]), keeps[0] * keeps[1]
+    n23, a23 = n_of(ns[2], keeps[2], ns[3], keeps[3]), keeps[2] * keeps[3]
+    n, a = n_of(n01, a01, n23, a23), a01 * a23
 
     def keep_rows(keep, qrow):
         hi = keep.astype(bf16).astype(f32)
@@ -329,7 +331,6 @@
         qrow = qrow + jnp.where(lane1 == 4 * sp + i, q4[:, i : i + 1], 0.0)
     xs[mx, 0:R, :] = lo(n)
     xs[mx, R : R + 16, :] = keep_rows(a, qrow)
-    bfull[...] = lo(b).reshape(NX, 32, R)
     sent_x = []
     for o in (2, 1, 3):
         c = pltpu.make_async_remote_copy(
@@ -338,6 +339,16 @@
         )
         c.start()
         sent_x.append(c)
+    bs = values()
+
+    def b_of(b1, n2, a2, b2):
+        return a2 * b1 - nn(lo(b1), lo(n2)) + b2
+
+    b01 = b_of(bs[0], ns[1], keeps[1], bs[1])
+    b23 = b_of(bs[2], ns[3], keeps[3], bs[3])
+    b = b_of(b01, n23, a23, b23)
+    bfull[...] = lo(b).reshape(NX, 32, R)
+    for o in (2, 1, 3):
         c = pltpu.make_async_remote_copy(
             bfull.at[(mx + o) % NX], xs.at[mx, pl.ds(R + 16, 32)],
             xsend.at[1, o - 1], xrecv.at[1, o - 1], device_id=at_x(o), device_id_type=MESH,

time: 61.2 us -> 60.6 us (level)
  the two profiles are of different devices: /device:TPU:2 before, /device:TPU:8 now
where the time goes in v3:
time: 60.6 us; the launch traced here: 60.4 us
  Pallas kernels  59.8 us (99%)
  between operations  0.64 us (1%)
    pallas_call x1, Pallas kernels, per_device(): pl.pallas_call(kernel, out_shape=jax.ShapeDtypeStruct((8, R), f32), in_sp...  58.5 us
    pallas_call x1, Pallas kernels, per_device(): pl.pallas_call(unpack_out, out_shape=(jax.ShapeDtypeStruct((1, 4, R), bf1...  1.25 us

profile of v3, /device:TPU:8, one launch (start us, length us, event | category | flops | bytes accessed | tf_op | source)
XLA Modules:
  0.0 60.4 jit_solution(18165161870550620950)
XLA Ops:
  0.6 58.5 %shard_map.113.packed = f32[8,128]{1,0:T(8,128)} custom-call(bf16[512,256]{1,0:T(8,128)(2,1)} %tok.1, bf16[4096,128]{1,0:T(8,128)(2,1)} %wk.1, bf16[4096,128]{1,0:T(8,128)(2,1)} %wv.1, bf16[16,4096]{1,0:T(8,128)(2,1)} %bitcast.3, bf16[16,4096]{1,0:T(8,128)(2,1)} %bitcast.4, f32[16]{0:T(128)} %bias_in.1, f32[16]{0:T(128)} %rate_in.1, f32[1,512]{1,0:T(1,128)} %finc_in.1, ...), custom_call_target="tpu_custom_call" | custom-call | tf_op jit(solution)/shard_map/pallas_call | solution.py:460
  59.1 1.3 %shard_map.114 = (bf16[1,4,128]{2,1,0:T(4,128)(2,1)}, f32[1,128]{1,0:T(1,128)}) custom-call(f32[8,128]{1,0:T(8,128)} %shard_map.113.packed), custom_call_target="tpu_custom_call" | custom-call | tf_op jit(solution)/shard_map/pallas_call | solution.py:497

commit v4 on v3

--- a/solution.py
+++ b/solution.py
@@ -459,7 +459,7 @@
     dma = pltpu.SemaphoreType.DMA
     packed = pl.pallas_call(
         kernel,
-        out_shape=jax.ShapeDtypeStruct((8, R), f32),
+        out_shape=pltpu.VMEM((8, R), f32),
         in_specs=[hbm] * 10,
         out_specs=vmem,
         scratch_shapes=[
@@ -502,7 +502,7 @@
         ),
         in_specs=[vmem],
         out_specs=(vmem, vmem),
-    )(packed)
+    )(pltpu.with_memory_space_constraint(packed, pltpu.VMEM))
 
 
 def solution(mesh):

time: 60.6 us -> 59.3 us (0.979)
  Pallas kernels: 59.8 us -> 58.5 us
    pallas_call x1, Pallas kernels: 1.25 us -> 0.57 us  [per_device(): pl.pallas_call(unpack_out, out_shape=(jax.ShapeDtypeStruct((1, 4, R), bf1...]
where the time goes in v4:
time: 59.3 us; the launch traced here: 59.1 us
  Pallas kernels  58.5 us (99%)
  between operations  0.64 us (1%)
    pallas_call x1, Pallas kernels, per_device(): pl.pallas_call(kernel, out_shape=pltpu.VMEM((8, R), f32), in_specs=[hbm]...  57.9 us

profile of v4, /device:TPU:8, one launch (start us, length us, event | category | flops | bytes accessed | tf_op | source)
XLA Modules:
  0.0 59.1 jit_solution(4901131779978189093)
XLA Ops:
  0.6 57.9 %shard_map.113.packed = f32[8,128]{1,0:T(8,128)S(1)} custom-call(bf16[512,256]{1,0:T(8,128)(2,1)} %tok.1, bf16[4096,128]{1,0:T(8,128)(2,1)} %wk.1, bf16[4096,128]{1,0:T(8,128)(2,1)} %wv.1, bf16[16,4096]{1,0:T(8,128)(2,1)} %bitcast.3, bf16[16,4096]{1,0:T(8,128)(2,1)} %bitcast.4, f32[16]{0:T(128)} %bias_in.1, f32[16]{0:T(128)} %rate_in.1, f32[1,512]{1,0:T(1,128)} %finc_in.1, ...), custom_call_target="tpu_custom_call" | custom-call | tf_op jit(solution)/shard_map/pallas_call | solution.py:460
  58.6 0.6 shard_map.114

commit v5 on v4

--- a/solution.py
+++ b/solution.py
@@ -52,10 +52,11 @@
 def block_maps(kvs, gates, fincs, bias, rate):
     count = len(kvs)
     row, col = iota((R, R), 0), iota((R, R), 1)
-    strict = row > col
+    strict = row < col
     eye = (row == col).astype(f32)
     kw = [kv[:, :R].astype(bf16) for kv in kvs]
-    kk = [nt(k, k) for k in kw]
+    kw_t = [k.T for k in kw]
+    kk = [nn(k, t) for k, t in zip(kw, kw_t)]
     logits = jnp.concatenate([dl for _, dl in gates] + [bl for bl, _ in gates], axis=0)
     c = -rate * jax.nn.softplus(logits) + jnp.concatenate(fincs + fincs, axis=0)
     beta = jax.nn.sigmoid(logits + bias)
@@ -79,8 +80,8 @@
     rs_r = [rs_rows[i : i + 1] for i in range(count)]
     lower = []
     for i in range(count):
-        decay = jnp.exp(jnp.where(strict, cum_c[i] - cum_r[i], 0.0))
-        lower.append(jnp.where(strict, kk[i] * (rs[i] * beta_c[i]) * rs_r[i] * decay, 0.0))
+        decay = jnp.exp(jnp.where(strict, cum_r[i] - cum_c[i], 0.0))
+        lower.append(jnp.where(strict, kk[i] * rs[i] * (rs_r[i] * beta_r[i]) * decay, 0.0))
     same = (row // 16) == (col // 16)
     power = [lo(jnp.where(same, l, 0.0)) for l in lower]
     inverse = [eye - jnp.where(same, l, 0.0) for l in lower]
@@ -89,7 +90,7 @@
         inverse = [x + nn(lo(x), p) for x, p in zip(inverse, power)]
     size = 16
     while size < R:
-        below = ((row // (2 * size)) == (col // (2 * size))) & ((row // size) > (col // size))
+        below = ((row // (2 * size)) == (col // (2 * size))) & ((row // size) < (col // size))
         short = [lo(x) for x in inverse]
         inner = [lo(nn(s, lo(jnp.where(below, l, 0.0)))) for s, l in zip(short, lower)]
         inverse = [x - nn(y, s) for x, y, s in zip(inverse, inner, short)]
@@ -99,14 +100,14 @@
         last = cum_r[i][:, R - 1 : R]
         keeps.append(jnp.broadcast_to(jnp.exp(last), (1, R)))
         remainders.append(lo(kw[i].astype(f32) * (rs[i] * jnp.exp(last - cum_c[i]))))
-        erase = nn(lo(inverse[i] * (beta_r[i] * jnp.exp(cum_r[i]) * rs_r[i])), kw[i])
-        ns.append(tn(lo(erase), remainders[i]))
+        erase_t = nn(kw_t[i], lo(inverse[i] * (beta_c[i] * jnp.exp(cum_c[i]) * rs[i])))
+        ns.append(nn(lo(erase_t), remainders[i]))
 
     def values():
         bs = []
         for i in range(count):
-            update = nn(lo(inverse[i] * beta_r[i]), kvs[i][:, R:].astype(bf16))
-            bs.append(tn(lo(update), remainders[i]))
+            update_t = nn(kvs[i][:, R:].astype(bf16).T, lo(inverse[i] * beta_c[i]))
+            bs.append(nn(lo(update_t), remainders[i]))
         return bs
 
     return ns, keeps, values
@@ -332,7 +333,7 @@
     xs[mx, 0:R, :] = lo(n)
     xs[mx, R : R + 16, :] = keep_rows(a, qrow)
     sent_x = []
-    for o in (2, 1, 3):
+    for o in (1, 3, 2):
         c = pltpu.make_async_remote_copy(
             xs.at[mx, pl.ds(0, R + 16)], xs.at[mx, pl.ds(0, R + 16)],
             xsend.at[0, o - 1], xrecv.at[0, o - 1], device_id=at_x(o), device_id_type=MESH,
@@ -348,13 +349,15 @@
     b23 = b_of(bs[2], ns[3], keeps[3], bs[3])
     b = b_of(b01, n23, a23, b23)
     bfull[...] = lo(b).reshape(NX, 32, R)
-    for o in (2, 1, 3):
+    for o in (1, 3, 2):
         c = pltpu.make_async_remote_copy(
             bfull.at[(mx + o) % NX], xs.at[mx, pl.ds(R + 16, 32)],
             xsend.at[1, o - 1], xrecv.at[1, o - 1], device_id=at_x(o), device_id_type=MESH,
         )
         c.start()
         sent_x.append(c)
+    for c in sent:
+        c.wait_send()
     xs[mx, R + 16 : R + 48, :] = bfull[mx]
 
     def unpack(ref, k):
@@ -402,28 +405,35 @@
 
     mine = mz // 2
     put(zs, mine, n, b, a, qrow)
-    for o in (3, 2, 1):
+    for o in (1, 2, 3):
         c = pltpu.make_async_remote_copy(
             zs.at[mine], zs.at[mine], zsend.at[o - 1], zrecv.at[o - 1],
             device_id=at_z(o * sigma), device_id_type=MESH,
         )
         c.start()
         sent_x.append(c)
-    for o, step in ((1, 1), (2, -2), (3, 3)):
-        src = ((mz + step * sigma + NZ) % NZ) // 2
-        pltpu.make_async_remote_copy(
-            zs.at[src], zs.at[src], zsend.at[o - 1], zrecv.at[o - 1],
-            device_id=at_z(o * sigma), device_id_type=MESH,
-        ).wait_recv()
-    got = [unpack(zs, k) for k in range(4)]
-    state = got[0][0][0][R:]
-    for k in range(1, 4):
-        nb, keep, nb_lo = got[k][0]
-        state = keep * state - nn(lo(state), nb_lo[:R]) + nb[R:]
-    qrow = got[0][1] + got[1][1] + got[2][1] + got[3][1]
+    state, qrow = None, None
+    for k in range(4):
+        d = (k - mine + 4) % 4
+        near = ((d + 3) // 2 + 1 - mz % 2) % 2
+        index = (d % 2) * near + (1 - d % 2) * 2
+
+        @pl.when(d != 0)
+        def _():
+            pltpu.make_async_remote_copy(
+                zs.at[k], zs.at[k], zsend.at[index], zrecv.at[index],
+                device_id=at_z(sigma), device_id_type=MESH,
+            ).wait_recv()
+
+        (nb, keep, nb_lo), q_part = unpack(zs, k)
+        if k == 0:
+            state, qrow = nb[R:], q_part
+        else:
+            state = keep * state - nn(lo(state), nb_lo[:R]) + nb[R:]
+            qrow = qrow + q_part
 
     fs[mx] = lo(state)
-    for o in (2, 1, 3):
+    for o in (1, 3, 2):
         c = pltpu.make_async_remote_copy(
             fs.at[mx], fs.at[mx], fsend.at[o - 1], frecv.at[o - 1],
             device_id=at_x(o), device_id_type=MESH,
@@ -444,7 +454,7 @@
     packed[0:4, :] = srow[pl.ds(pl.multiple_of(4 * sp, 4), 4), :]
     packed[4:5, :] = read
 
-    for c in sent + sent_x:
+    for c in sent_x:
         c.wait_send()
 
 

time: 59.3 us -> 58.6 us (0.988)
  the two profiles are of different devices: /device:TPU:8 before, /device:TPU:2 now
where the time goes in v5:
time: 58.6 us; the launch traced here: 58.4 us
  Pallas kernels  57.8 us (99%)
  between operations  0.64 us (1%)
    pallas_call x1, Pallas kernels, per_device(): pl.pallas_call(kernel, out_shape=pltpu.VMEM((8, R), f32), in_specs=[hbm]...  57.2 us

profile of v5, /device:TPU:2, one launch (start us, length us, event | category | flops | bytes accessed | tf_op | source)
XLA Modules:
  0.0 58.4 jit_solution(8592636242094844673)
XLA Ops:
  0.6 57.2 %shard_map.113.packed = f32[8,128]{1,0:T(8,128)S(1)} custom-call(bf16[512,256]{1,0:T(8,128)(2,1)} %tok.1, bf16[4096,128]{1,0:T(8,128)(2,1)} %wk.1, bf16[4096,128]{1,0:T(8,128)(2,1)} %wv.1, bf16[16,4096]{1,0:T(8,128)(2,1)} %bitcast.3, bf16[16,4096]{1,0:T(8,128)(2,1)} %bitcast.4, f32[16]{0:T(128)} %bias_in.1, f32[16]{0:T(128)} %rate_in.1, f32[1,512]{1,0:T(1,128)} %finc_in.1, ...), custom_call_target="tpu_custom_call" | custom-call | tf_op jit(solution)/shard_map/pallas_call | solution.py:470
  57.8 0.6 shard_map.114
